TPU v7x, 32 devices: a whole 2x2x4 slice. The times are simulated.
32 devices in a mesh: sp: 8 (over z, y), tp: 4 (over x, core).
Axes of the slice: x: 2, y: 2, z: 4, core: 2. Of those that a mesh axis runs over, the one named last changes fastest.
Arguments:
- stream_in: bfloat16 [2048, 4096], P(('sp', 'tp')), may hold values from -6 to 6
- q_first: bfloat16 [2048, 1024], P('sp', 'tp'), may hold values from -110 to 110
- q_second: bfloat16 [2048, 1024], P('sp', 'tp'), may hold values from -110 to 110
- k_first: bfloat16 [2048, 512], P('sp', 'tp'), may hold values from -7 to 7
- k_second: bfloat16 [2048, 512], P('sp', 'tp'), may hold values from -7 to 7
- values: bfloat16 [2048, 1024], P('sp', 'tp'), may hold values from -6 to 6
- head_lambda: float32 [8], P('tp'), may hold values from 0.3 to 0.8
- w_out: bfloat16 [2048, 4096], P('tp'), may hold values from -0.125 to 0.125
- norm_gain: float32 [4096], replicated, may hold values from 0.1 to 1.9
- routes: int32 [2048, 4], P(('sp', 'tp')), may hold values from 0 to 7, all different within a row; in each aligned block of 64 rows (0 to 63, 64 to 127, ...) at most 48 rows name the same one
- route_w: float32 [2048, 4], P(('sp', 'tp')), may hold values from 0.2 to 1
- w_gate: bfloat16 [8, 4096, 128], P('sp'), may hold values from -0.09375 to 0.09375
- w_up: bfloat16 [8, 4096, 128], P('sp'), may hold values from -0.09375 to 0.09375
- w_down: bfloat16 [8, 128, 4096], P('sp'), may hold values from -0.5 to 0.5
- s_gate: bfloat16 [4096, 512], P(None, 'tp'), may hold values from -0.09375 to 0.09375
- s_up: bfloat16 [4096, 512], P(None, 'tp'), may hold values from -0.09375 to 0.09375
- s_down: bfloat16 [512, 4096], P('tp'), may hold values from -0.25 to 0.25
Outputs:
- layer_out: bfloat16 [2048, 4096], P(('sp', 'tp'))
Inputs may be any that keep to these rules, and one draw needn't show every extreme that they name: `routes`: each row names 4 different experts. Within the rows of one device (aligned blocks of 64 rows) no expert is named more than 48 times, and in some blocks one expert is named exactly 48 times.
All inputs are finite; a program needn't handle non-finite values.
Results may differ from a plain program's by a relative error of at most 0.017.
Values may be sent and summed in bfloat16 or wider, within the bound.
A program may use at most 128 MiB of HBM per device.

v0:
```python
import math

import jax
import jax.numpy as jnp
from jax import lax
from jax.sharding import PartitionSpec as P

HEAD = 128


FLOOR = -1e30


def absorb(state, first_q, second_q, first_k, second_k, value_rows, query_pos, key_pos):
    allowed = key_pos[None, :] <= query_pos[:, None]
    scale = first_q.shape[-1] ** (-0.5)
    result = []
    pairs = ((first_q, first_k), (second_q, second_k))
    for index in range(2):
        query_rows, key_rows = pairs[index]
        peak, total, accum = (state[3 * index], state[3 * index + 1], state[3 * index + 2])
        scores = (
            jnp.einsum("qagd,kad->agqk", query_rows, key_rows, preferred_element_type=jnp.float32)
            * scale
        )
        scores = jnp.where(allowed, scores, FLOOR)
        raised = jnp.maximum(peak, scores.max(-1))
        weights = jnp.where(allowed, jnp.exp(scores - raised[..., None]), 0.0)
        fade = jnp.exp(peak - raised)
        total = total * fade + weights.sum(-1)
        accum = accum * fade[..., None] + jnp.einsum(
            "agqk,kad->agqd",
            weights.astype(jnp.bfloat16),
            value_rows,
            preferred_element_type=jnp.float32,
        )
        result += [raised, total, accum]
    return tuple(result)


def empty_state(kv_local, group, count, value_dim):
    peaks = jnp.full((kv_local, group, count), FLOOR, jnp.float32)
    sums = jnp.zeros((kv_local, group, count), jnp.float32)
    accums = jnp.zeros((kv_local, group, count, value_dim), jnp.float32)
    return (peaks, sums, accums, peaks, sums, accums)


def fold_rows(state, first_q, second_q, query_pos, last_row, pieces, start):
    first_k, second_k, value_rows = pieces
    length = first_k.shape[0]
    kv_local = first_q.shape[1]
    value_dim = value_rows.shape[1] // kv_local
    span = math.gcd(length, 2048)

    def sweep(current):

        def visit(block, inner):
            begin = block * span
            key_one = lax.dynamic_slice_in_dim(first_k, begin, span, 0).reshape(
                span, kv_local, HEAD
            )
            key_two = lax.dynamic_slice_in_dim(second_k, begin, span, 0).reshape(
                span, kv_local, HEAD
            )
            value_part = lax.dynamic_slice_in_dim(value_rows, begin, span, 0).reshape(
                span, kv_local, value_dim
            )
            key_pos = begin + jnp.arange(span, dtype=jnp.int32)
            return absorb(
                inner, first_q, second_q, key_one, key_two, value_part, query_pos, key_pos
            )

        return lax.fori_loop(0, length // span, visit, current)

    def unchanged(current):
        return current

    return lax.cond(start <= last_row, sweep, unchanged, state)


def finish_heads(final, head_lambda):
    kv_local, group, count, value_dim = final[2].shape
    weight = head_lambda.reshape(kv_local, group, 1, 1)
    head_out = final[2] / final[1][..., None] - weight * final[5] / final[4][..., None]
    head_out = head_out * lax.rsqrt(jnp.mean(head_out * head_out, axis=-1, keepdims=True) + 1e-05)
    return (
        head_out.transpose(2, 0, 1, 3)
        .reshape(count, kv_local * group * value_dim)
        .astype(jnp.bfloat16)
    )


def shared_part(normed, s_gate, s_up, s_down):
    piece = lax.all_gather(normed, "tp", axis=0, tiled=True)
    gate_part = jnp.dot(piece, s_gate, preferred_element_type=jnp.float32)
    up_part = jnp.dot(piece, s_up, preferred_element_type=jnp.float32)
    hidden = (jax.nn.silu(gate_part) * up_part).astype(jnp.bfloat16)
    terms = jnp.dot(hidden, s_down, preferred_element_type=jnp.float32)
    return lax.psum_scatter(
        terms.astype(jnp.bfloat16), "tp", scatter_dimension=0, tiled=True
    ).astype(jnp.float32)


def routed_part(normed, routes, route_w, w_gate, w_up, w_down):
    rows, topk = routes.shape
    local_experts = w_gate.shape[0]
    experts = local_experts * lax.axis_size("sp")
    slots = max(2, 3 * rows * topk // (2 * experts))
    flat_ids = routes.reshape(-1)
    hits = (flat_ids[:, None] == jnp.arange(experts, dtype=jnp.int32)[None, :]).astype(jnp.int32)
    slot_of = jnp.sum(jnp.cumsum(hits, axis=0) * hits, axis=1) - 1
    target = flat_ids * slots + slot_of
    placing = jnp.any(
        jnp.arange(experts * slots, dtype=jnp.int32)[:, None, None]
        == target.reshape(rows, topk)[None, :, :],
        axis=-1,
    ).astype(jnp.bfloat16)
    outgoing = (
        jnp.dot(placing, normed, preferred_element_type=jnp.float32)
        .astype(jnp.bfloat16)
        .reshape(experts, slots, normed.shape[1])
    )
    arrived = lax.all_to_all(outgoing, "sp", split_axis=0, concat_axis=0, tiled=True)
    sources = arrived.shape[0] // local_experts
    grouped = arrived.reshape(sources, local_experts, arrived.shape[1], arrived.shape[2])
    gate_part = jnp.einsum("sjcd,jdf->sjcf", grouped, w_gate, preferred_element_type=jnp.float32)
    up_part = jnp.einsum("sjcd,jdf->sjcf", grouped, w_up, preferred_element_type=jnp.float32)
    hidden = (jax.nn.silu(gate_part) * up_part).astype(jnp.bfloat16)
    result = jnp.einsum(
        "sjcf,jfd->sjcd", hidden, w_down, preferred_element_type=jnp.float32
    ).astype(jnp.bfloat16)
    returned = lax.all_to_all(
        result.reshape(arrived.shape), "sp", split_axis=0, concat_axis=0, tiled=True
    )
    picked = (
        returned.reshape(experts * slots, normed.shape[1])[target]
        .reshape(rows, topk, normed.shape[1])
        .astype(jnp.float32)
    )
    return jnp.sum(picked * route_w[..., None], axis=1)


def local(
    stream_in,
    q_first,
    q_second,
    k_first,
    k_second,
    values,
    head_lambda,
    w_out,
    norm_gain,
    routes,
    route_w,
    w_gate,
    w_up,
    w_down,
    s_gate,
    s_up,
    s_down,
):
    seq_rows = q_first.shape[0]
    kv_local = k_first.shape[1] // HEAD
    heads_local = q_first.shape[1] // HEAD
    group = heads_local // kv_local
    value_dim = values.shape[1] // kv_local
    offset = lax.axis_index("sp") * seq_rows
    query_pos = offset + jnp.arange(seq_rows, dtype=jnp.int32)
    last_row = offset + seq_rows - 1
    first_q = q_first.reshape(seq_rows, kv_local, group, HEAD)
    second_q = q_second.reshape(seq_rows, kv_local, group, HEAD)
    start_state = empty_state(kv_local, group, seq_rows, value_dim)
    folded_state = fold_rows(
        start_state,
        first_q,
        second_q,
        query_pos,
        last_row,
        (
            lax.all_gather(k_first, "sp", axis=0, tiled=True),
            lax.all_gather(k_second, "sp", axis=0, tiled=True),
            lax.all_gather(values, "sp", axis=0, tiled=True),
        ),
        jnp.int32(0),
    )
    attn_rows = finish_heads(folded_state, head_lambda)
    attn = lax.psum_scatter(
        jnp.dot(attn_rows, w_out, preferred_element_type=jnp.float32).astype(jnp.bfloat16),
        "tp",
        scatter_dimension=0,
        tiled=True,
    ).astype(jnp.float32)
    resid = (stream_in.astype(jnp.float32) + attn).astype(jnp.bfloat16)
    stream = lax.optimization_barrier(resid).astype(jnp.float32)
    normed = (
        stream * lax.rsqrt(jnp.mean(stream * stream, axis=-1, keepdims=True) + 1e-06) * norm_gain
    ).astype(jnp.bfloat16)
    routed = routed_part(normed, routes, route_w, w_gate, w_up, w_down)
    shared = shared_part(normed, s_gate, s_up, s_down)
    return (stream + routed + shared).astype(jnp.bfloat16)


def solution(mesh):
    return jax.shard_map(
        local,
        mesh=mesh,
        in_specs=(
            P(("sp", "tp"), None),
            P("sp", "tp"),
            P("sp", "tp"),
            P("sp", "tp"),
            P("sp", "tp"),
            P("sp", "tp"),
            P("tp"),
            P("tp", None),
            P(),
            P(("sp", "tp"), None),
            P(("sp", "tp"), None),
            P("sp", None, None),
            P("sp", None, None),
            P("sp", None, None),
            P(None, "tp"),
            P(None, "tp"),
            P("tp", None),
        ),
        out_specs=P(("sp", "tp"), None),
        check_vma=False,
    )
```

profile of v0, /device:TPU:0, one launch (start us, length us, event | category | flops | bytes accessed | tf_op | source)
XLA Modules:
  0.0 313.2 jit_solution(3209219373579061836)
XLA Ops:
  6.5 0.7 all-gather.3.cloned.1.call-update
  7.3 0.0 reduce-scatter.3.cloned.1.call-start
  7.3 33.8 %all_gather.12 = bf16[2048,128]{1,0:T(8,128)(2,1)S(1)} all-gather(bf16[256,128]{1,0:T(8,128)(2,1)} %param.22), channel_id=1, replica_groups=mesh['sp'=8,'tp'=4] {'sp'}, dimensions={0}, use_global_device_ids=true | all-gather | bytes 589824 | tf_op jit(solution)/shard_map/all_gather | solution.py:180
  41.1 32.0 %all_gather.14 = bf16[2048,128]{1,0:T(8,128)(2,1)S(1)} all-gather(bf16[256,128]{1,0:T(8,128)(2,1)} %param.23), channel_id=1, replica_groups=mesh['sp'=8,'tp'=4] {'sp'}, dimensions={0}, use_global_device_ids=true | all-gather | bytes 589824 | tf_op jit(solution)/shard_map/all_gather | solution.py:181
  73.1 12.4 %conditional.1 = (f32[1,2,256]{2,1,0:T(2,128)S(1)}, f32[1,2,256]{2,1,0:T(2,128)S(1)}, f32[1,2,256,256]{2,3,1,0:T(8,128)S(1)}, f32[1,2,256,256]{2,3,1,0:T(8,128)}) conditional(s32[]{:T(128)} %convert_element_type.75, () %tuple.15, (s32[]{:T(128)}, s32[256]{0:T(256)S(1)}, bf16[256,256]{1,0:T(8,128)(2,1)}, bf16[2048,128]{1,0:T(8,128)(2,1)S(1)}, ...), branch_computations={%region_0.0_spmd, %region_1.6_spmd} | conditional | flops 1638665472 | bytes 60079224 | solution.py:78
  73.1 0.3 iota_compare_fusion
  73.5 1.6 fusion.30
  75.1 1.5 fusion.1
  76.6 0.4 copy-done.1
  77.0 2.1 fusion.5
  79.1 1.5 fusion.17
  80.6 1.0 copy.52
  81.6 3.6 %fusion.23 = f32[1,2,256,256]{3,2,1,0:T(8,128)S(1)} fusion(f32[2048,256,2]{1,0,2:T(8,128)} %copy-done.1, f32[2,256]{1,0:T(2,128)S(1)} %broadcast_maximum_fusion.1, pred[256,2048]{0,1:T(8,128)(4,1)S(1)} %iota_compare_fusion, bf16[2048,256]{1,0:T(8,128)(2,1)S(1)} %copy-done.13, f32[2,256]{1,0:T(2,128)S(1)} %get-tuple-element.98), kind=kOutput, calls=%fused_computation.21 | convolution fusion | flops 542244864 | bytes 6295552 | tf_op jit(solution)/shard_map/cond/branch_1_fun/while/body/eval_jaxpr/agqk,kad->agqd/dot_general | solution.py:31
  85.3 0.2 copy.50
  85.5 1.2 multiply_reduce_fusion.1
  86.8 4.9 %convolution_convert_fusion.3 = bf16[256,4096]{1,0:T(8,128)(2,1)} fusion(bf16[256,512]{0,1:T(8,128)(2,1)S(1)} %bitcast.154, bf16[512,4096]{1,0:T(8,128)(2,1)} %param.26), kind=kOutput, calls=%fused_computation.48 | convolution fusion | flops 1074790400 | bytes 6553600 | tf_op jit(solution)/shard_map/dot_general | solution.py:188
  91.7 0.1 copy.42
  91.8 0.1 eq.43
  91.9 0.1 eq.39
  92.0 0.6 reduce-window.6
  92.6 0.2 slice_reduce_fusion
  92.9 0.1 fusion.69
  93.0 0.1 sub.77
  93.1 0.1 copy.45
  93.2 0.1 fusion.56
  93.3 30.8 %reduce-scatter.3.cloned.1.call-done = bf16[64,4096]{1,0:T(8,128)(2,1)} async-done(((bf16[256,4096]{1,0:T(8,128)(2,1)}), bf16[64,4096]{1,0:T(8,128)(2,1)}) %reduce-scatter.3.cloned.1.call-update) | async-done | bytes 524304 | tf_op jit(solution)/shard_map/reduce_scatter | solution.py:187
  124.1 1.2 add_convert_fusion
  125.3 0.2 fusion.46
  125.5 0.6 copy-done.3
  126.1 0.2 fusion.48
  126.3 2.7 convolution_convert_fusion
  129.0 5.7 %all-to-all-start = ((bf16[8,48,4096]{2,1,0:T(8,128)(2,1)}), bf16[8,48,4096]{2,1,0:T(8,128)(2,1)}, u32[]{:S(2)}, u32[]{:S(2)}) async-start(bf16[8,48,4096]{2,1,0:T(8,128)(2,1)} %bitcast.153), calls=%async_computation.1 | async-start | bytes 6291456 | tf_op jit(solution)/shard_map/all_to_all | solution.py:123
  134.6 0.2 all-gather.5.cloned.1.call-start
  134.8 0.5 all-gather.5.cloned.1.call-update
  135.4 69.9 %all-to-all-done = bf16[8,48,4096]{2,1,0:T(8,128)(2,1)} async-done(((bf16[8,48,4096]{2,1,0:T(8,128)(2,1)}), bf16[8,48,4096]{2,1,0:T(8,128)(2,1)}, u32[]{:S(2)}, u32[]{:S(2)}) %all-to-all-start) | async-done | bytes 3145760 | tf_op jit(solution)/shard_map/all_to_all | solution.py:123
  205.3 2.9 convolution_bitcast_fusion.1
  208.1 7.3 %convolution_convert_fusion.1 = bf16[8,48,4096]{2,1,0:T(8,128)(2,1)} fusion(bf16[1,128,4096]{2,1,0:T(8,128)(2,1)S(1)} %copy-done, bf16[8,48,4096]{2,1,0:T(8,128)(2,1)} %all-to-all-done, bf16[1,4096,128]{2,1,0:T(8,128)(2,1)} %param.31, f32[8,1,48,128]{3,2,0,1:T(8,128)S(1)} %convolution_bitcast_fusion.1), kind=kOutput, calls=%fused_computation.46 | convolution fusion | flops 807174144 | bytes 8585216 | tf_op jit(solution)/shard_map/sjcf,jfd->sjcd/dot_general | solution.py:129
  215.4 4.4 %all-to-all-start.1 = ((bf16[8,48,4096]{2,1,0:T(8,128)(2,1)}), bf16[8,48,4096]{2,1,0:T(8,128)(2,1)}, u32[]{:S(2)}, u32[]{:S(2)}) async-start(bf16[8,48,4096]{2,1,0:T(8,128)(2,1)} %convolution_convert_fusion.1), calls=%async_computation.2 | async-start | bytes 6291456 | tf_op jit(solution)/shard_map/all_to_all | solution.py:132
  219.9 0.0 reduce-scatter.5.cloned.1.call-start
  219.9 2.7 fusion.74
  222.7 4.2 %convolution_convert_fusion.2 = bf16[256,4096]{1,0:T(8,128)(2,1)} fusion(bf16[128,4096]{1,0:T(8,128)(2,1)} %param.35, bf16[256,4096]{1,0:T(8,128)(2,1)S(1)} %copy-done.2, bf16[4096,128]{1,0:T(8,128)(2,1)} %param.34, f32[256,128]{1,0:T(8,128)S(1)} %fusion.74), kind=kOutput, calls=%fused_computation.47 | convolution fusion | flops 538116096 | bytes 6422528 | tf_op jit(solution)/shard_map/dot_general | solution.py:98
  226.9 0.1 mul.180
  227.0 0.1 copy.46
  227.1 62.9 %all-to-all-done.1 = bf16[8,48,4096]{2,1,0:T(8,128)(2,1)} async-done(((bf16[8,48,4096]{2,1,0:T(8,128)(2,1)}), bf16[8,48,4096]{2,1,0:T(8,128)(2,1)}, u32[]{:S(2)}, u32[]{:S(2)}) %all-to-all-start.1) | async-done | bytes 3145760 | tf_op jit(solution)/shard_map/all_to_all | solution.py:132
  290.0 6.2 %gather_fusion = bf16[256,4096]{1,0:T(8,128)(2,1)S(1)} fusion(bf16[384,4096]{1,0:T(8,128)(2,1)} %bitcast.35, s32[1024]{0:T(1024)S(1)} %pad_clamp_fusion), kind=kCustom, calls=%fused_computation | custom fusion | bytes 4195328 | tf_op jit(solution)/shard_map/gather | solution.py:136
  296.2 3.0 reshape.284
  299.3 5.3 %multiply_reduce_fusion = f32[64,4096]{1,0:T(8,128)S(1)} fusion(f32[64,4,4096]{2,1,0:T(4,128)} %reshape.284, f32[64,4]{1,0:T(8,128)S(1)} %copy.46), kind=kLoop, calls=%fused_computation.49 | loop fusion | flops 1835008 | bytes 5243904 | tf_op jit(solution)/shard_map/reduce_sum | solution.py:140
  304.7 2.0 fusion.50
  (47 shorter events, 0.3 us)
Async XLA Ops:
  6.5 201.6 %copy-start = (bf16[1,128,4096]{2,1,0:T(8,128)(2,1)S(1)}, bf16[1,128,4096]{2,1,0:T(8,128)(2,1)}, u32[]{:S(2)}) copy-start(bf16[1,128,4096]{2,1,0:T(8,128)(2,1)} %param.32) | copy-start | bytes 3145732
  6.5 66.5 %all-gather.3.cloned.1.call-start = ((), (), s32[]{:S(2)}) async-start(), calls=%async_computation.4 | async-start | bytes 1179648 | tf_op jit(solution)/shard_map/all_gather | solution.py:182
  7.3 116.8 %reduce-scatter.3.cloned.1.call-start = ((), (), s32[]{:S(2)}) async-start(), calls=%async_computation.5 | async-start | bytes 2621440 | tf_op jit(solution)/shard_map/reduce_scatter | solution.py:187
  73.1 12.4 %copy-start.12 = (f32[2]{0:T(128)S(1)}, f32[2]{0:T(128)}, u32[]{:S(2)}) copy-start(f32[2]{0:T(128)} %param.25) | copy-start | bytes 28
  73.1 2.0 copy-start.8
  75.1 1.9 copy-start.1
  77.0 2.1 copy-start.13
  86.8 4.9 %copy-start.10 = (s32[64,4]{0,1:T(4,128)S(1)}, s32[64,4]{0,1:T(4,128)}, u32[]{:S(2)}) copy-start(s32[64,4]{0,1:T(4,128)} %param.28) | copy-start | bytes 3076
  86.8 37.3 %copy-start.7 = (bf16[64,4096]{1,0:T(8,128)(2,1)S(1)}, bf16[64,4096]{1,0:T(8,128)(2,1)}, u32[]{:S(2)}) copy-start(bf16[64,4096]{1,0:T(8,128)(2,1)} %param.19) | copy-start | bytes 1572868
  86.8 39.3 %copy-start.9 = (f32[4096]{0:T(1024)S(1)}, f32[4096]{0:T(1024)}, u32[]{:S(2)}) copy-start(f32[4096]{0:T(1024)} %param.27) | copy-start | bytes 49156
  125.3 0.8 copy-start.3
  126.3 2.7 copy-start.5
  129.0 76.3 %copy-start.6 = (bf16[1,4096,128]{2,1,0:T(8,128)(2,1)S(1)}, bf16[1,4096,128]{2,1,0:T(8,128)(2,1)}, u32[]{:S(2)}) copy-start(bf16[1,4096,128]{2,1,0:T(8,128)(2,1)} %param.30) | copy-start | bytes 3145732
  129.0 76.3 %all-to-all-start = ((bf16[8,48,4096]{2,1,0:T(8,128)(2,1)}), bf16[8,48,4096]{2,1,0:T(8,128)(2,1)}, u32[]{:S(2)}, u32[]{:S(2)}) async-start(bf16[8,48,4096]{2,1,0:T(8,128)(2,1)} %bitcast.153), calls=%async_computation.1 | async-start | bytes 6291456 | tf_op jit(solution)/shard_map/all_to_all | solution.py:123
  134.6 85.3 %all-gather.5.cloned.1.call-start = ((), (), s32[]{:S(2)}) async-start(), calls=%async_computation.6 | async-start | bytes 2621440 | tf_op jit(solution)/shard_map/all_gather | solution.py:94
  215.4 74.6 %all-to-all-start.1 = ((bf16[8,48,4096]{2,1,0:T(8,128)(2,1)}), bf16[8,48,4096]{2,1,0:T(8,128)(2,1)}, u32[]{:S(2)}, u32[]{:S(2)}) async-start(bf16[8,48,4096]{2,1,0:T(8,128)(2,1)} %convolution_convert_fusion.1), calls=%async_computation.2 | async-start | bytes 6291456 | tf_op jit(solution)/shard_map/all_to_all | solution.py:132
  219.9 84.8 %reduce-scatter.5.cloned.1.call-start = ((), (), s32[]{:S(2)}) async-start(), calls=%async_computation.7 | async-start | bytes 2621440 | tf_op jit(solution)/shard_map/reduce_scatter | solution.py:99
  219.9 2.7 copy-start.2
  222.7 4.4 %copy-start.11 = (f32[64,4]{0,1:T(4,128)S(1)}, f32[64,4]{0,1:T(4,128)}, u32[]{:S(2)}) copy-start(f32[64,4]{0,1:T(4,128)} %param.29) | copy-start | bytes 3076
  299.3 5.4 %copy-start.4 = (bf16[64,4096]{1,0:T(8,128)(2,1)S(1)}, bf16[64,4096]{1,0:T(8,128)(2,1)}, u32[]{:S(2)}) copy-start(bf16[64,4096]{1,0:T(8,128)(2,1)} %copy-done.3) | copy-start | bytes 1572868
Sparse Core Ops, SparseCore 0:
  9.5 45.9 all-gather.2
  91.8 32.2 reduce-scatter.2
  137.0 23.0 all-gather.4
  227.0 31.4 reduce-scatter.4
where the time goes:
time: 314 us; the launch traced here: 313 us
  waiting for transfers between devices  165 us (53%)
  blocking collectives  65.8 us (21%)
  matrix products  32.8 us (10%)
  other arithmetic  13.5 us (4%)
  between operations  13.4 us (4%)
  local copies, waits for them, and re-layouts  12.3 us (4%)
  starting transfers between devices  10.4 us (3%)
    all_to_all x1, waiting for transfers between devices, routed_part(): lax.all_to_all(outgoing, 'sp', split_axis=0, concat_axis=0, tiled=True)  69.9 us
    all_to_all x1, waiting for transfers between devices, routed_part(): lax.all_to_all(result.reshape(arrived.shape), 'sp', split_axis=0, concat_...  62.9 us
    all_gather x1, blocking collectives, local(): lax.all_gather(k_first, 'sp', axis=0, tiled=True)  33.8 us
    all_gather x1, blocking collectives, local(): lax.all_gather(k_second, 'sp', axis=0, tiled=True)  32 us
    reduce_scatter x1, waiting for transfers between devices, local(): lax.psum_scatter(jnp.dot(attn_rows, w_out, preferred_element_type=jnp.flo...  30.8 us
    dot_general x1, matrix products, routed_part(): jnp.einsum('sjcf,jfd->sjcd', hidden, w_down, preferred_element_type=jnp.f...  7.26 us
  transfers between devices with their start and end apart: 6, of which 3 were waited for; matrix products, arithmetic and copies ran while one was open for 11% of the time, Pallas kernels for 0%

commit v1 on v0

--- a/solution.py
+++ b/solution.py
@@ -1,8 +1,11 @@
+import functools
 import math
 
 import jax
 import jax.numpy as jnp
 from jax import lax
+from jax.experimental import pallas as pl
+from jax.experimental.pallas import tpu as pltpu
 from jax.sharding import PartitionSpec as P
 
 HEAD = 128
@@ -200,9 +203,592 @@
     return (stream + routed + shared).astype(jnp.bfloat16)
 
 
+def mesh_copy(src, dst, send_sem, recv_sem, axis, target):
+    return pltpu.make_async_remote_copy(
+        src_ref=src,
+        dst_ref=dst,
+        send_sem=send_sem,
+        recv_sem=recv_sem,
+        device_id={axis: target},
+        device_id_type=pl.DeviceIdType.MESH,
+    )
+
+
+def greet(axis, target):
+    pl.semaphore_signal(
+        pltpu.get_barrier_semaphore(),
+        inc=1,
+        device_id={axis: target},
+        device_id_type=pl.DeviceIdType.MESH,
+    )
+
+
+def attend_kernel(
+    n,
+    group,
+    q_one,
+    q_two,
+    k_one,
+    k_two,
+    val,
+    lam,
+    out,
+    stacked,
+    keys_one,
+    keys_two,
+    vals,
+    peak,
+    total,
+    accum,
+    send_sem,
+    recv_sem,
+):
+    me = lax.axis_index("sp")
+    place, side = me // 2, me % 2
+    depth = n // 2
+    pair = me + 1 - 2 * side
+    above = place < depth - 1
+    rows = q_one.shape[0]
+    sources = (k_one, k_two, val)
+    held = (keys_one, keys_two, vals)
+    scale = HEAD ** (-0.5)
+
+    @pl.when(place > 0)
+    def _():
+        greet("sp", me - 2)
+
+    @pl.when(above)
+    def _():
+        greet("sp", me + 2)
+
+    greet("sp", pair)
+    pl.semaphore_wait(
+        pltpu.get_barrier_semaphore(),
+        1 + (place > 0).astype(jnp.int32) + above.astype(jnp.int32),
+    )
+
+    def copies(block, way, target, own):
+        return [
+            mesh_copy(
+                sources[a] if own else held[a].at[block],
+                held[a].at[block],
+                send_sem.at[way, a, block],
+                recv_sem.at[a, block],
+                "sp",
+                target,
+            )
+            for a in range(3)
+        ]
+
+    def start(block, way, target, own=False):
+        for one in copies(block, way, target, own):
+            one.start()
+
+    def arrive(block):
+        for one in copies(block, 0, pair, False):
+            one.wait_recv()
+
+    @pl.when(above)
+    def _():
+        start(me, 0, me + 2, True)
+
+    @pl.when(side == 0)
+    def _():
+        start(me, 1, pair, True)
+
+    for index, q in enumerate((q_one, q_two)):
+        for h in range(group):
+            stacked[index, h * rows : (h + 1) * rows, :] = q[:, h * HEAD : (h + 1) * HEAD]
+
+    def scores_of(index, keys):
+        return (
+            lax.dot_general(
+                stacked[index], keys, (((1,), (1,)), ((), ())), preferred_element_type=jnp.float32
+            )
+            * scale
+        )
+
+    spread = (group * rows, rows)
+    row_of = lax.broadcasted_iota(jnp.int32, spread, 0) % rows
+    allowed = lax.broadcasted_iota(jnp.int32, spread, 1) <= row_of
+    for index, keys in enumerate((k_one, k_two)):
+        scores = jnp.where(allowed, scores_of(index, keys[...]), FLOOR)
+        top = jnp.max(scores, axis=-1, keepdims=True)
+        weights = jnp.exp(scores - top)
+        peak[index] = top
+        total[index] = jnp.sum(weights, axis=-1, keepdims=True)
+        accum[index] = jnp.dot(
+            weights.astype(jnp.bfloat16), val[...], preferred_element_type=jnp.float32
+        )
+
+    def fold(block):
+        for index in range(2):
+            scores = scores_of(index, held[index][block])
+            old = peak[index]
+            top = jnp.maximum(old, jnp.max(scores, axis=-1, keepdims=True))
+            weights = jnp.exp(scores - top)
+            fade = jnp.exp(old - top)
+            peak[index] = top
+            total[index] = total[index] * fade + jnp.sum(weights, axis=-1, keepdims=True)
+            accum[index] = accum[index] * fade + jnp.dot(
+                weights.astype(jnp.bfloat16), vals[block], preferred_element_type=jnp.float32
+            )
+
+    def visit(e, carry):
+        @pl.when(place >= e)
+        def _():
+            block = me - 2 * e
+            arrive(block)
+
+            @pl.when(above)
+            def _():
+                start(block, 0, me + 2)
+
+            start(block, 1, pair)
+            fold(block)
+
+        @pl.when((place >= e - 1) & ((e > 1) | (side == 1)))
+        def _():
+            block = pair - 2 * (e - 1)
+            arrive(block)
+            fold(block)
+
+        return carry
+
+    lax.fori_loop(1, depth + 1, visit, 0)
+
+    for h in range(group):
+        part = slice(h * rows, (h + 1) * rows)
+        head = accum[0, part, :] / total[0, part, :] - lam[h] * (
+            accum[1, part, :] / total[1, part, :]
+        )
+        head = head * lax.rsqrt(jnp.mean(head * head, axis=-1, keepdims=True) + 1e-05)
+        width = head.shape[1]
+        out[:, h * width : (h + 1) * width] = head.astype(jnp.bfloat16)
+
+    def settle(e, carry):
+        @pl.when(place >= e)
+        def _():
+            block = me - 2 * e
+
+            @pl.when(above)
+            def _():
+                for one in copies(block, 0, me + 2, False):
+                    one.wait_send()
+
+            @pl.when((e > 0) | (side == 0))
+            def _():
+                for one in copies(block, 1, pair, False):
+                    one.wait_send()
+
+        return carry
+
+    lax.fori_loop(0, depth, settle, 0)
+
+
+def attend(n, q_first, q_second, k_first, k_second, values, head_lambda):
+    rows = q_first.shape[0]
+    group = q_first.shape[1] // HEAD
+    value_dim = values.shape[1]
+    vmem = pl.BlockSpec(memory_space=pltpu.VMEM)
+    tall = group * rows
+    flops = 4 * tall * n * rows * (HEAD + value_dim)
+    return pl.pallas_call(
+        functools.partial(attend_kernel, n, group),
+        out_shape=jax.ShapeDtypeStruct((rows, group * value_dim), jnp.bfloat16),
+        in_specs=[vmem] * 5 + [pl.BlockSpec(memory_space=pltpu.SMEM)],
+        out_specs=vmem,
+        scratch_shapes=[
+            pltpu.VMEM((2, tall, HEAD), jnp.bfloat16),
+            pltpu.VMEM((n, rows, HEAD), jnp.bfloat16),
+            pltpu.VMEM((n, rows, HEAD), jnp.bfloat16),
+            pltpu.VMEM((n, rows, value_dim), jnp.bfloat16),
+            pltpu.VMEM((2, tall, 1), jnp.float32),
+            pltpu.VMEM((2, tall, 1), jnp.float32),
+            pltpu.VMEM((2, tall, value_dim), jnp.float32),
+            pltpu.SemaphoreType.DMA((2, 3, n)),
+            pltpu.SemaphoreType.DMA((3, n)),
+        ],
+        compiler_params=pltpu.CompilerParams(collective_id=0, has_side_effects=True),
+        cost_estimate=pl.CostEstimate(flops=flops * 8, bytes_accessed=1 << 24, transcendentals=0),
+        name="attend",
+    )(q_first, q_second, k_first, k_second, values, head_lambda)
+
+
+def project_kernel(
+    nt, pieces, rows_in, w, stream, gain, resid, normed, order, out_one, in_one, out_two, in_two,
+    send_one, recv_one, send_two, recv_two,
+):
+    me = lax.axis_index("tp")
+    far, near = me // 2, me % 2
+    partner = me + 1 - 2 * near
+    half = nt // 2
+    rows = stream.shape[0]
+    wide = w.shape[1] // pieces
+    greet("tp", partner)
+    for o in range(1, half):
+        greet("tp", 2 * ((far + o) % half) + near)
+    pl.semaphore_wait(pltpu.get_barrier_semaphore(), half)
+
+    for o in range(half):
+        base = 2 * ((far + o) % half)
+        for which, parity in enumerate((1 - near, near)):
+            begin = pl.multiple_of((base + parity) * rows, rows)
+            order[which, o * rows : (o + 1) * rows, :] = rows_in[pl.ds(begin, rows), :]
+
+    first = [
+        mesh_copy(out_one.at[i], in_one.at[i], send_one.at[i], recv_one.at[i], "tp", partner)
+        for i in range(pieces)
+    ]
+    second = [
+        [
+            mesh_copy(
+                out_two.at[o, i],
+                in_two.at[o, i],
+                send_two.at[o, i],
+                recv_two.at[o, i],
+                "tp",
+                2 * ((far + o + 1) % half) + near,
+            )
+            for o in range(half - 1)
+        ]
+        for i in range(pieces)
+    ]
+    for i in range(pieces):
+        column = slice(i * wide, (i + 1) * wide)
+        out_one[i] = jnp.dot(
+            order[0], w[:, column], preferred_element_type=jnp.float32
+        ).astype(jnp.bfloat16)
+        first[i].start()
+    kept = []
+    for i in range(pieces):
+        column = slice(i * wide, (i + 1) * wide)
+        part = jnp.dot(order[1], w[:, column], preferred_element_type=jnp.float32)
+        first[i].wait_recv()
+        part = part + in_one[i].astype(jnp.float32)
+        for o in range(half - 1):
+            out_two[o, i] = part[(o + 1) * rows : (o + 2) * rows].astype(jnp.bfloat16)
+            second[i][o].start()
+        kept.append(part[:rows])
+    squares = jnp.zeros((rows, 1), jnp.float32)
+    for i in range(pieces):
+        column = slice(i * wide, (i + 1) * wide)
+        part = kept[i]
+        for o in range(half - 1):
+            second[i][o].wait_recv()
+            part = part + in_two[o, i].astype(jnp.float32)
+        sums = (stream[:, column].astype(jnp.float32) + part).astype(jnp.bfloat16)
+        resid[:, column] = sums
+        sums = sums.astype(jnp.float32)
+        squares = squares + jnp.sum(sums * sums, axis=-1, keepdims=True)
+    shrink = lax.rsqrt(squares / stream.shape[1] + 1e-06)
+    for i in range(pieces):
+        column = slice(i * wide, (i + 1) * wide)
+        normed[:, column] = (
+            resid[:, column].astype(jnp.float32) * shrink * gain[:, column]
+        ).astype(jnp.bfloat16)
+    for i in range(pieces):
+        first[i].wait_send()
+        for o in range(half - 1):
+            second[i][o].wait_send()
+
+
+def project(nt, attn_rows, w_out, stream_in, norm_gain):
+    rows, width = stream_in.shape
+    pieces = 4
+    wide = width // pieces
+    half = nt // 2
+    vmem = pl.BlockSpec(memory_space=pltpu.VMEM)
+    shape = jax.ShapeDtypeStruct((rows, width), jnp.bfloat16)
+    flops = 2 * attn_rows.shape[0] * attn_rows.shape[1] * width
+    return pl.pallas_call(
+        functools.partial(project_kernel, nt, pieces),
+        out_shape=(shape, shape),
+        in_specs=[vmem] * 4,
+        out_specs=(vmem, vmem),
+        scratch_shapes=[
+            pltpu.VMEM((2, half * rows, attn_rows.shape[1]), jnp.bfloat16),
+            pltpu.VMEM((pieces, half * rows, wide), jnp.bfloat16),
+            pltpu.VMEM((pieces, half * rows, wide), jnp.bfloat16),
+            pltpu.VMEM((half - 1, pieces, rows, wide), jnp.bfloat16),
+            pltpu.VMEM((half - 1, pieces, rows, wide), jnp.bfloat16),
+            pltpu.SemaphoreType.DMA((pieces,)),
+            pltpu.SemaphoreType.DMA((pieces,)),
+            pltpu.SemaphoreType.DMA((half - 1, pieces)),
+            pltpu.SemaphoreType.DMA((half - 1, pieces)),
+        ],
+        compiler_params=pltpu.CompilerParams(collective_id=1, has_side_effects=True),
+        cost_estimate=pl.CostEstimate(flops=flops * 8, bytes_accessed=1 << 24, transcendentals=0),
+        name="project",
+    )(attn_rows, w_out, stream_in, norm_gain.reshape(1, width))
+
+
+def hidden_kernel(
+    n, nt, x, gate, up, s_gate, s_up, mix, out, gathered, beside, out_hid, in_hid, out_sh, in_sh,
+    send_x, recv_x, send_b, recv_b, send_h, recv_h, send_s, recv_s,
+):
+    me, mine = lax.axis_index("sp"), lax.axis_index("tp")
+    place, side = me // 2, me % 2
+    depth = n // 2
+    pair = me + 1 - 2 * side
+    above, below = place < depth - 1, place > 0
+    hid = gate.shape[1]
+    for o in range(1, n):
+        greet("sp", (me + o) % n)
+    for o in range(1, nt):
+        greet("tp", (mine + o) % nt)
+    pl.semaphore_wait(pltpu.get_barrier_semaphore(), n + nt - 2)
+
+    def row_copy(block, way, target, own=False):
+        return mesh_copy(
+            x if own else gathered.at[block],
+            gathered.at[block],
+            send_x.at[way, block],
+            recv_x.at[block],
+            "sp",
+            target,
+        )
+
+    def hid_copy(block):
+        return mesh_copy(
+            out_hid.at[block], in_hid.at[me], send_h.at[block], recv_h.at[me], "sp", block
+        )
+
+    def hid_arrival(block):
+        return mesh_copy(
+            out_hid.at[block], in_hid.at[block], send_h.at[block], recv_h.at[block], "sp", block
+        )
+
+    @pl.when(above)
+    def _():
+        row_copy(me, 0, me + 2, True).start()
+
+    @pl.when(below)
+    def _():
+        row_copy(me, 1, me - 2, True).start()
+
+    row_copy(me, 2, pair, True).start()
+    side_copies = [
+        mesh_copy(
+            x, beside.at[o - 1], send_b.at[o - 1], recv_b.at[o - 1], "tp", (mine + o) % nt
+        )
+        for o in range(1, nt)
+    ]
+    for one in side_copies:
+        one.start()
+
+    def hidden_of(block_rows, g, u):
+        gate_part = jnp.dot(block_rows, g[...], preferred_element_type=jnp.float32)
+        up_part = jnp.dot(block_rows, u[...], preferred_element_type=jnp.float32)
+        return (gate_part / (1.0 + jnp.exp(-gate_part)) * up_part).astype(jnp.bfloat16)
+
+    in_hid[me] = hidden_of(x[...], gate, up)
+    in_sh[mine] = hidden_of(x[...], s_gate, s_up)
+
+    def serve(block):
+        out_hid[block] = hidden_of(gathered[block], gate, up)
+        hid_copy(block).start()
+
+    shared_copies = [
+        mesh_copy(
+            out_sh.at[o - 1],
+            in_sh.at[mine],
+            send_s.at[o - 1],
+            recv_s.at[mine],
+            "tp",
+            (mine + nt - o) % nt,
+        )
+        for o in range(1, nt)
+    ]
+
+    def visit(e, carry):
+        low, high = place >= e, place + e < depth
+
+        @pl.when(low)
+        def _():
+            block = me - 2 * e
+            row_copy(block, 0, pair).wait_recv()
+
+            @pl.when(above)
+            def _():
+                row_copy(block, 0, me + 2).start()
+
+            row_copy(block, 2, pair).start()
+
+        @pl.when(high)
+        def _():
+            block = me + 2 * e
+            row_copy(block, 0, pair).wait_recv()
+
+            @pl.when(below)
+            def _():
+                row_copy(block, 1, me - 2).start()
+
+            row_copy(block, 2, pair).start()
+
+        @pl.when(low)
+        def _():
+            serve(me - 2 * e)
+
+        @pl.when(high)
+        def _():
+            serve(me + 2 * e)
+
+        @pl.when(place >= e - 1)
+        def _():
+            block = pair - 2 * (e - 1)
+            row_copy(block, 0, pair).wait_recv()
+            serve(block)
+
+        @pl.when((e > 1) & (place + e - 1 < depth))
+        def _():
+            block = pair + 2 * (e - 1)
+            row_copy(block, 0, pair).wait_recv()
+            serve(block)
+
+        @pl.when(e == depth - 1)
+        def _():
+            for o in range(1, nt):
+                side_copies[o - 1].wait_recv()
+                out_sh[o - 1] = hidden_of(beside[o - 1], s_gate, s_up)
+                shared_copies[o - 1].start()
+
+        return carry
+
+    lax.fori_loop(1, depth + 1, visit, 0)
+
+    for o in range(1, n):
+        hid_arrival((me + o) % n).wait_recv()
+    for o in range(1, nt):
+        source = (mine + o) % nt
+        mesh_copy(
+            out_sh.at[o - 1], in_sh.at[source], send_s.at[o - 1], recv_s.at[source], "tp", source
+        ).wait_recv()
+    for j in range(n):
+        out[:, j * hid : (j + 1) * hid] = (
+            in_hid[j].astype(jnp.float32) * mix[:, j : j + 1]
+        ).astype(jnp.bfloat16)
+    wide = s_gate.shape[1]
+    for j in range(nt):
+        out[:, n * hid + j * wide : n * hid + (j + 1) * wide] = in_sh[j]
+
+    def settle(block, carry):
+        spot = block // 2
+
+        @pl.when(block % 2 == side)
+        def _():
+            row_copy(block, 2, pair).wait_send()
+
+            @pl.when(above & (spot <= place))
+            def _():
+                row_copy(block, 0, me + 2).wait_send()
+
+            @pl.when(below & (spot >= place))
+            def _():
+                row_copy(block, 1, me - 2).wait_send()
+
+        @pl.when(block != me)
+        def _():
+            hid_copy(block).wait_send()
+
+        return carry
+
+    lax.fori_loop(0, n, settle, 0)
+    for o in range(1, nt):
+        side_copies[o - 1].wait_send()
+        shared_copies[o - 1].wait_send()
+
+
+def hidden_units(n, nt, normed, w_gate, w_up, s_gate, s_up, mix):
+    rows, width = normed.shape
+    hid, wide = w_gate.shape[1], s_gate.shape[1]
+    vmem = pl.BlockSpec(memory_space=pltpu.VMEM)
+    flops = 4 * rows * width * (n * hid + nt * wide)
+    return pl.pallas_call(
+        functools.partial(hidden_kernel, n, nt),
+        out_shape=jax.ShapeDtypeStruct((rows, n * hid + nt * wide), jnp.bfloat16),
+        in_specs=[vmem] * 6,
+        out_specs=vmem,
+        scratch_shapes=[
+            pltpu.VMEM((n, rows, width), jnp.bfloat16),
+            pltpu.VMEM((nt - 1, rows, width), jnp.bfloat16),
+            pltpu.VMEM((n, rows, hid), jnp.bfloat16),
+            pltpu.VMEM((n, rows, hid), jnp.bfloat16),
+            pltpu.VMEM((nt - 1, rows, wide), jnp.bfloat16),
+            pltpu.VMEM((nt, rows, wide), jnp.bfloat16),
+            pltpu.SemaphoreType.DMA((3, n)),
+            pltpu.SemaphoreType.DMA((n,)),
+            pltpu.SemaphoreType.DMA((nt - 1,)),
+            pltpu.SemaphoreType.DMA((nt - 1,)),
+            pltpu.SemaphoreType.DMA((n,)),
+            pltpu.SemaphoreType.DMA((n,)),
+            pltpu.SemaphoreType.DMA((nt - 1,)),
+            pltpu.SemaphoreType.DMA((nt,)),
+        ],
+        compiler_params=pltpu.CompilerParams(collective_id=2, has_side_effects=True),
+        cost_estimate=pl.CostEstimate(flops=flops * 40, bytes_accessed=1 << 24, transcendentals=0),
+        name="hidden_units",
+    )(normed, w_gate, w_up, s_gate, s_up, mix)
+
+
+def near(
+    stream_in,
+    q_first,
+    q_second,
+    k_first,
+    k_second,
+    values,
+    head_lambda,
+    w_out,
+    norm_gain,
+    routes,
+    route_w,
+    w_gate,
+    w_up,
+    w_down,
+    s_gate,
+    s_up,
+    s_down,
+):
+    n, nt = lax.axis_size("sp"), lax.axis_size("tp")
+    hid, wide = w_down.shape[1], s_down.shape[0]
+    routed_piece = lax.dynamic_slice_in_dim(
+        w_down[0], lax.axis_index("tp") * (hid // nt), hid // nt, 0
+    )
+    shared_piece = lax.dynamic_slice_in_dim(
+        s_down, lax.axis_index("sp") * (wide // n), wide // n, 0
+    )
+    routed_down = lax.all_gather(routed_piece, ("sp", "tp"), axis=0, tiled=True)
+    shared_down = lax.all_gather(shared_piece, ("tp", "sp"), axis=0, tiled=True)
+    attn_rows = attend(n, q_first, q_second, k_first, k_second, values, head_lambda)
+    resid, normed = project(nt, attn_rows, w_out, stream_in, norm_gain)
+    chosen = routes[:, :, None] == jnp.arange(n, dtype=jnp.int32)[None, None, :]
+    mix = jnp.sum(jnp.where(chosen, route_w[:, :, None], 0.0), axis=1)
+    units = hidden_units(n, nt, normed, w_gate[0], w_up[0], s_gate, s_up, mix)
+    routed = jnp.dot(units[:, : n * hid], routed_down, preferred_element_type=jnp.float32)
+    shared = jnp.dot(units[:, n * hid :], shared_down, preferred_element_type=jnp.float32)
+    return (resid.astype(jnp.float32) + routed + shared).astype(jnp.bfloat16)
+
+
+def layer(*arrays):
+    n, nt = lax.axis_size("sp"), lax.axis_size("tp")
+    k_first, values, w_gate, w_down, s_down = (arrays[i] for i in (3, 5, 11, 13, 16))
+    fits = (
+        2 <= n <= 16
+        and n % 2 == 0
+        and nt >= 4
+        and nt % 2 == 0
+        and k_first.shape[1] == HEAD
+        and w_gate.shape[0] == 1
+        and w_down.shape[1] % (16 * nt) == 0
+        and s_down.shape[0] % (16 * n) == 0
+    )
+    return near(*arrays) if fits else local(*arrays)
+
+
 def solution(mesh):
     return jax.shard_map(
-        local,
+        layer,
         mesh=mesh,
         in_specs=(
             P(("sp", "tp"), None),

time: 314 us -> 184 us (0.59)
  waiting for transfers between devices: 165 us -> 18.4 us
  Pallas kernels: 0 us -> 139 us
  blocking collectives: 65.8 us -> 0 us
  matrix products: 32.8 us -> 8.89 us
  other arithmetic: 13.5 us -> 0.71 us
  starting transfers between devices: 10.4 us -> 0.04 us
  local copies, waits for them, and re-layouts: 12.3 us -> 4.2 us
    pallas_call x0 -> x3, Pallas kernels: none -> 139 us  [the longest x1 107 us: hidden_units(): pl.pallas_call(functools.partial(hidden_kernel, n, nt), out_shape=jax.Sha...]
    all_to_all x2 -> x0, waiting for transfers between devices: 133 us -> none  [the longest x1 69.9 us: routed_part(): lax.all_to_all(outgoing, 'sp', split_axis=0, concat_axis=0, tiled=True)]
    all_gather x2 -> x0, blocking collectives: 65.8 us -> none  [the longest x1 33.8 us: local(): lax.all_gather(k_first, 'sp', axis=0, tiled=True)]
    reduce_scatter x2 -> x0, waiting for transfers between devices: 30.8 us -> none  [the longest x1 30.8 us: local(): lax.psum_scatter(jnp.dot(attn_rows, w_out, preferred_element_type=jnp.flo...]
    dot_general x10 -> x2, matrix products: 32.8 us -> 8.89 us  [the longest x1 5.03 us: near(): jnp.dot(units[:, :n * hid], routed_down, preferred_element_type=jnp.float32)]
    all_gather x2, waiting for transfers between devices: 0.02 us -> 18.3 us  [the longest x1 18.3 us: near(): shared_down = lax.all_gather(shared_piece, ('tp', 'sp'), axis=0, tiled=True)]
    all_to_all x2 -> x0, starting transfers between devices: 10.1 us -> none  [the longest x1 5.65 us: routed_part(): lax.all_to_all(outgoing, 'sp', split_axis=0, concat_axis=0, tiled=True)]
    reduce_sum x5 -> x1, other arithmetic: 8.95 us -> 0.71 us  [near(): mix = jnp.sum(jnp.where(chosen, route_w[:, :, None], 0.0), axis=1)]
  transfers between devices with their start and end apart: 6 -> 2, of which waited for: 3 -> 1; matrix products, arithmetic and copies ran while one was open for 11% -> 4% of each run, Pallas kernels for 0% -> 75%
where the time goes in v1:
time: 184 us
  Pallas kernels  139 us (76%)
  waiting for transfers between devices  18.4 us (10%)
  between operations  13.5 us (7%)
  matrix products  8.89 us (5%)
  local copies, waits for them, and re-layouts  4.2 us (2%)
    pallas_call x1, Pallas kernels, hidden_units(): pl.pallas_call(functools.partial(hidden_kernel, n, nt), out_shape=jax.Sha...  107 us
    pallas_call x1, Pallas kernels, project(): pl.pallas_call(functools.partial(project_kernel, nt, pieces), out_shape=(...  20.1 us
    all_gather x1, waiting for transfers between devices, near(): shared_down = lax.all_gather(shared_piece, ('tp', 'sp'), axis=0, tiled=True)  18.3 us
    pallas_call x1, Pallas kernels, attend(): pl.pallas_call(functools.partial(attend_kernel, n, group), out_shape=jax....  11.1 us
    dot_general x1, matrix products, near(): jnp.dot(units[:, :n * hid], routed_down, preferred_element_type=jnp.float32)  5.03 us
    dot_general x1, matrix products, near(): jnp.dot(units[:, n * hid:], shared_down, preferred_element_type=jnp.float32)  3.87 us
  transfers between devices with their start and end apart: 2, of which 1 were waited for; matrix products, arithmetic and copies ran while one was open for 4% of the time, Pallas kernels for 75%

profile of v1, /device:TPU:0, one launch (start us, length us, event | category | flops | bytes accessed | tf_op | source)
XLA Modules:
  0.0 184.2 jit_solution(6342147371613666346)
XLA Ops:
  6.5 0.0 copy-start
  6.5 0.0 all-gather.6.cloned.1.call-start
  6.5 1.2 copy-done
  7.8 0.7 constant_dynamic-slice_fusion.1
  8.5 0.0 all-gather.6.cloned.1.call-update
  8.5 0.0 all-gather.4.cloned.1.call-start
  8.6 1.6 constant_dynamic-slice_fusion
  10.1 0.0 all-gather.4.cloned.1.call-update
  10.2 0.7 select_reduce_fusion
  10.9 0.7 copy.20.mix
  11.6 11.1 %attend.1.rows_in = bf16[256,512]{1,0:T(8,128)(2,1)} custom-call(bf16[256,256]{1,0:T(8,128)(2,1)} %q_one.1, bf16[256,256]{1,0:T(8,128)(2,1)} %q_two.1, bf16[256,128]{1,0:T(8,128)(2,1)} %k_one.1, bf16[256,128]{1,0:T(8,128)(2,1)} %k_two.1, bf16[256,256]{1,0:T(8,128)(2,1)} %val.1, f32[2]{0:T(128)} %lam.1), custom_call_target="tpu_custom_call" | custom-call | flops 12884901888 | bytes 16777216 | tf_op jit(solution)/shard_map/attend/pallas_call | solution.py:396
  22.6 20.1 %project.1 = (bf16[64,4096]{1,0:T(8,128)(2,1)}, bf16[64,4096]{1,0:T(8,128)(2,1)}) custom-call(bf16[256,512]{1,0:T(8,128)(2,1)} %attend.1.rows_in, bf16[512,4096]{1,0:T(8,128)(2,1)} %w.1, bf16[64,4096]{1,0:T(8,128)(2,1)} %stream.1, f32[1,4096]{1,0:T(1,128)} %bitcast.11), custom_call_target="tpu_custom_call" | custom-call | flops 8589934592 | bytes 16777216 | tf_op jit(solution)/shard_map/project/pallas_call | solution.py:504
  42.8 0.0 copy-start.1
  42.8 107.4 %hidden_units.1 = bf16[64,1536]{1,0:T(8,128)(2,1)} custom-call(bf16[64,4096]{1,0:T(8,128)(2,1)} %get-tuple-element.8.x, bf16[4096,128]{1,0:T(8,128)(2,1)} %bitcast.9, bf16[4096,128]{1,0:T(8,128)(2,1)} %bitcast.10, bf16[4096,128]{1,0:T(8,128)(2,1)} %s_gate.1, bf16[4096,128]{1,0:T(8,128)(2,1)} %s_up.1, f32[64,8]{1,0:T(8,128)} %copy.20.mix), custom_call_target="tpu_custom_call" | custom-call | flops 64424509440 | bytes 16777216 | tf_op jit(solution)/shard_map/hidden_units/pallas_call | solution.py:707
  150.1 0.0 all-gather.6.cloned.1.call-done
  150.2 0.0 copy-done.1
  150.2 5.0 %fusion.2 = f32[64,4096]{1,0:T(8,128)S(1)} fusion(bf16[1,1024,4096]{2,1,0:T(8,128)(2,1)} %all-gather.6.cloned.1.call-done, bf16[64,4096]{1,0:T(8,128)(2,1)S(1)} %copy-done.1, bf16[64,1536]{1,0:T(8,128)(2,1)} %hidden_units.1), kind=kOutput, calls=%fused_computation.3 | convolution fusion | flops 537395200 | bytes 10092544 | tf_op jit(solution)/shard_map/dot_general | solution.py:768
  155.2 18.3 %all-gather.4.cloned.1.call-done = bf16[512,4096]{1,0:T(8,128)(2,1)} async-done(((bf16[16,4096]{1,0:T(8,128)(2,1)}), bf16[512,4096]{1,0:T(8,128)(2,1)}) %all-gather.4.cloned.1.call-update) | async-done | bytes 4194320 | tf_op jit(solution)/shard_map/all_gather | solution.py:762
  173.5 3.9 %fusion.5 = bf16[64,4096]{1,0:T(8,128)(2,1)} fusion(f32[64,4096]{1,0:T(8,128)S(1)} %fusion.2, bf16[512,4096]{1,0:T(8,128)(2,1)} %all-gather.4.cloned.1.call-done, bf16[64,1536]{1,0:T(8,128)(2,1)} %hidden_units.1), kind=kOutput, calls=%fused_computation.4 | convolution fusion | flops 268959744 | bytes 5832704 | tf_op jit(solution)/shard_map/dot_general | solution.py:769
Async XLA Ops:
  6.5 1.2 copy-start
  6.5 143.6 %all-gather.6.cloned.1.call-start = ((), (), s32[]{:S(2)}) async-start(), calls=%async_computation.1 | async-start | bytes 8650752 | tf_op jit(solution)/shard_map/all_gather | solution.py:761
  8.5 165.0 %all-gather.4.cloned.1.call-start = ((), (), s32[]{:S(2)}) async-start(), calls=%async_computation | async-start | bytes 4325376 | tf_op jit(solution)/shard_map/all_gather | solution.py:762
  42.8 107.4 %copy-start.1 = (bf16[64,4096]{1,0:T(8,128)(2,1)S(1)}, bf16[64,4096]{1,0:T(8,128)(2,1)}, u32[]{:S(2)}) copy-start(bf16[64,4096]{1,0:T(8,128)(2,1)} %get-tuple-element.7) | copy-start | bytes 1572868
Sparse Core Ops, SparseCore 0:
  10.2 90.6 all-gather.5
  104.0 69.5 all-gather.3

commit v2 on v0

--- a/solution.py
+++ b/solution.py
@@ -1,8 +1,11 @@
+import functools
 import math
 
 import jax
 import jax.numpy as jnp
 from jax import lax
+from jax.experimental import pallas as pl
+from jax.experimental.pallas import tpu as pltpu
 from jax.sharding import PartitionSpec as P
 
 HEAD = 128
@@ -200,9 +203,678 @@
     return (stream + routed + shared).astype(jnp.bfloat16)
 
 
+def mesh_copy(src, dst, send_sem, recv_sem, axis, target):
+    return pltpu.make_async_remote_copy(
+        src_ref=src,
+        dst_ref=dst,
+        send_sem=send_sem,
+        recv_sem=recv_sem,
+        device_id={axis: target},
+        device_id_type=pl.DeviceIdType.MESH,
+    )
+
+
+def greet(axis, target):
+    pl.semaphore_signal(
+        pltpu.get_barrier_semaphore(),
+        inc=1,
+        device_id={axis: target},
+        device_id_type=pl.DeviceIdType.MESH,
+    )
+
+
+def near_kernel(
+    n, nt, group, pieces,
+    q_one, q_two, k_one, k_two, val, lam, w_out_h, stream, gain, mix,
+    gate_h, up_h, s_gate_h, s_up_h, down_h, s_down_h,
+    out,
+    stacked, keys_one, keys_two, vals, peak, total, accum, rows_in,
+    w, order, out_one, in_one, out_two, in_two, resid,
+    gates, ups, s_gate, s_up, wall, gathered, beside, out_hid, in_hid, out_sh, in_sh, units,
+    load, send_kv, recv_kv, send_one, recv_one, send_two, recv_two,
+    send_g, recv_g, send_d, recv_d, send_sd, recv_sd,
+    send_x, recv_x, send_b, recv_b, send_h, recv_h, send_s, recv_s,
+):
+    me, mine = lax.axis_index("sp"), lax.axis_index("tp")
+    place, side = me // 2, me % 2
+    far, core = mine // 2, mine % 2
+    depth, half = n // 2, nt // 2
+    pair, partner = me + 1 - 2 * side, mine + 1 - 2 * core
+    above, below = place < depth - 1, place > 0
+    seq = q_one.shape[0]
+    rows, width = stream.shape
+    hid, wide = down_h.shape[0], s_down_h.shape[0]
+    scale = HEAD ** (-0.5)
+
+    def fars(o):
+        return 2 * ((far + o) % half) + core
+
+    def column(o):
+        return 2 * ((place + o) % depth) + side
+
+    loads = [
+        pltpu.make_async_copy(source, target, load.at[i])
+        for i, (source, target) in enumerate(
+            (
+                (w_out_h, w),
+                (gate_h, gates.at[0]),
+                (up_h, ups.at[0]),
+                (s_gate_h, s_gate),
+                (s_up_h, s_up),
+                (down_h, wall.at[pl.ds(pl.multiple_of(me * hid, hid), hid)]),
+                (s_down_h, wall.at[pl.ds(pl.multiple_of(n * hid + mine * wide, wide), wide)]),
+            )
+        )
+    ]
+    for o in range(1, depth):
+        greet("sp", column(o))
+    greet("sp", pair)
+    for o in range(1, half):
+        greet("tp", fars(o))
+    greet("tp", partner)
+    pl.semaphore_wait(pltpu.get_barrier_semaphore(), depth + half)
+
+    sources = (k_one, k_two, val)
+    held = (keys_one, keys_two, vals)
+
+    def copies(block, way, target, own):
+        return [
+            mesh_copy(
+                sources[a] if own else held[a].at[block],
+                held[a].at[block],
+                send_kv.at[way, a, block],
+                recv_kv.at[a, block],
+                "sp",
+                target,
+            )
+            for a in range(3)
+        ]
+
+    def start(block, way, target, own=False):
+        for one in copies(block, way, target, own):
+            one.start()
+
+    def arrive(block):
+        for one in copies(block, 0, pair, False):
+            one.wait_recv()
+
+    share = width // 2
+    share_at = pl.ds(pl.multiple_of(core * share, share), share)
+    other_at = pl.ds(pl.multiple_of((1 - core) * share, share), share)
+
+    def pair_weights():
+        return [
+            mesh_copy(
+                h.at[share_at], v.at[1, share_at], send_g.at[0, i], recv_g.at[0, i], "sp", pair
+            )
+            for i, (h, v) in enumerate(((gate_h, gates), (up_h, ups)))
+        ]
+
+    def pair_weights_on(at):
+        return [
+            mesh_copy(
+                v.at[1, at], v.at[1, at], send_g.at[1, i], recv_g.at[1, i], "tp", partner
+            )
+            for i, v in enumerate((gates, ups))
+        ]
+
+    part = hid // 2
+
+    def down_at(block, c):
+        return wall.at[pl.ds(pl.multiple_of(block * hid + c * part, part), part)]
+
+    def down_own(way, target, axis="sp"):
+        return mesh_copy(
+            down_h.at[pl.ds(pl.multiple_of(core * part, part), part)],
+            down_at(me, core),
+            send_d.at[way],
+            recv_d.at[0, me],
+            axis,
+            target,
+        )
+
+    def down_pair(block):
+        return mesh_copy(
+            down_at(block, core),
+            down_at(block, core),
+            send_d.at[depth + block],
+            recv_d.at[0, block],
+            "sp",
+            pair,
+        )
+
+    def down_core(block, c):
+        return mesh_copy(
+            down_at(block, c),
+            down_at(block, c),
+            send_d.at[depth + n + block],
+            recv_d.at[1, block],
+            "tp",
+            partner,
+        )
+
+    def sd_at(u):
+        return wall.at[pl.ds(pl.multiple_of(n * hid + u * wide, wide), wide)]
+
+    def sd_own(way, target):
+        return mesh_copy(s_down_h, sd_at(mine), send_sd.at[way], recv_sd.at[mine], "tp", target)
+
+    def sd_on(o, u):
+        return mesh_copy(
+            sd_at(u), sd_at(u), send_sd.at[half + o - 1], recv_sd.at[u], "tp", partner
+        )
+
+    @pl.when(above)
+    def _():
+        start(me, 0, me + 2, True)
+
+    @pl.when(side == 0)
+    def _():
+        start(me, 1, pair, True)
+
+    for one in loads:
+        one.start()
+    for o in range(1, half):
+        sd_own(o, fars(o)).start()
+    sd_own(0, partner).start()
+    for o in range(1, depth):
+
+        @pl.when(place + o >= depth)
+        def _():
+            down_own(o, column(o)).start()
+
+    for index, q in enumerate((q_one, q_two)):
+        for h in range(group):
+            stacked[index, h * seq : (h + 1) * seq, :] = q[:, h * HEAD : (h + 1) * HEAD]
+
+    def scores_of(index, keys):
+        return (
+            lax.dot_general(
+                stacked[index], keys, (((1,), (1,)), ((), ())), preferred_element_type=jnp.float32
+            )
+            * scale
+        )
+
+    spread = (group * seq, seq)
+    row_of = lax.broadcasted_iota(jnp.int32, spread, 0) % seq
+    allowed = lax.broadcasted_iota(jnp.int32, spread, 1) <= row_of
+    for index, keys in enumerate((k_one, k_two)):
+        scores = jnp.where(allowed, scores_of(index, keys[...]), FLOOR)
+        top = jnp.max(scores, axis=-1, keepdims=True)
+        weights = jnp.exp(scores - top)
+        peak[index] = top
+        total[index] = jnp.sum(weights, axis=-1, keepdims=True)
+        accum[index] = jnp.dot(
+            weights.astype(jnp.bfloat16), val[...], preferred_element_type=jnp.float32
+        )
+
+    def fold(block):
+        for index in range(2):
+            scores = scores_of(index, held[index][block])
+            old = peak[index]
+            top = jnp.maximum(old, jnp.max(scores, axis=-1, keepdims=True))
+            weights = jnp.exp(scores - top)
+            fade = jnp.exp(old - top)
+            peak[index] = top
+            total[index] = total[index] * fade + jnp.sum(weights, axis=-1, keepdims=True)
+            accum[index] = accum[index] * fade + jnp.dot(
+                weights.astype(jnp.bfloat16), vals[block], preferred_element_type=jnp.float32
+            )
+
+    def visit(e, carry):
+        @pl.when(place >= e)
+        def _():
+            block = me - 2 * e
+            arrive(block)
+
+            @pl.when(above)
+            def _():
+                start(block, 0, me + 2)
+
+            start(block, 1, pair)
+            fold(block)
+
+        @pl.when((place >= e - 1) & ((e > 1) | (side == 1)))
+        def _():
+            block = pair - 2 * (e - 1)
+            arrive(block)
+            fold(block)
+
+        @pl.when(e == jnp.maximum(place, 1))
+        def _():
+            for one in pair_weights():
+                one.start()
+            down_own(0, pair).start()
+
+        return carry
+
+    lax.fori_loop(1, depth + 1, visit, 0)
+
+    for o in range(1, depth):
+
+        @pl.when(place + o < depth)
+        def _():
+            down_own(o, column(o)).start()
+
+    for h in range(group):
+        cut = slice(h * seq, (h + 1) * seq)
+        head = accum[0, cut, :] / total[0, cut, :] - lam[h] * (
+            accum[1, cut, :] / total[1, cut, :]
+        )
+        head = head * lax.rsqrt(jnp.mean(head * head, axis=-1, keepdims=True) + 1e-05)
+        size = head.shape[1]
+        rows_in[:, h * size : (h + 1) * size] = head.astype(jnp.bfloat16)
+
+    for o in range(half):
+        base = 2 * ((far + o) % half)
+        for which, parity in enumerate((1 - core, core)):
+            begin = pl.multiple_of((base + parity) * rows, rows)
+            order[which, o * rows : (o + 1) * rows, :] = rows_in[pl.ds(begin, rows), :]
+
+    first = [
+        mesh_copy(out_one.at[i], in_one.at[i], send_one.at[i], recv_one.at[i], "tp", partner)
+        for i in range(pieces)
+    ]
+    second = [
+        [
+            mesh_copy(
+                out_two.at[o, i],
+                in_two.at[o, i],
+                send_two.at[o, i],
+                recv_two.at[o, i],
+                "tp",
+                fars(o + 1),
+            )
+            for o in range(half - 1)
+        ]
+        for i in range(pieces)
+    ]
+    span = width // pieces
+    loads[0].wait()
+    for i in range(pieces):
+        out_one[i] = jnp.dot(
+            order[0], w[:, i * span : (i + 1) * span], preferred_element_type=jnp.float32
+        ).astype(jnp.bfloat16)
+        first[i].start()
+    kept = []
+    for i in range(pieces):
+        sums = jnp.dot(
+            order[1], w[:, i * span : (i + 1) * span], preferred_element_type=jnp.float32
+        )
+        first[i].wait_recv()
+        sums = sums + in_one[i].astype(jnp.float32)
+        for o in range(half - 1):
+            out_two[o, i] = sums[(o + 1) * rows : (o + 2) * rows].astype(jnp.bfloat16)
+            second[i][o].start()
+        kept.append(sums[:rows])
+    squares = jnp.zeros((rows, 1), jnp.float32)
+    for i in range(pieces):
+        cut = slice(i * span, (i + 1) * span)
+        sums = kept[i]
+        for o in range(half - 1):
+            second[i][o].wait_recv()
+            sums = sums + in_two[o, i].astype(jnp.float32)
+        sums = (stream[:, cut].astype(jnp.float32) + sums).astype(jnp.bfloat16)
+        resid[:, cut] = sums
+        sums = sums.astype(jnp.float32)
+        squares = squares + jnp.sum(sums * sums, axis=-1, keepdims=True)
+    shrink = lax.rsqrt(squares / width + 1e-06)
+    for i in range(pieces):
+        cut = slice(i * span, (i + 1) * span)
+        gathered[place, :, cut] = (
+            resid[:, cut].astype(jnp.float32) * shrink * gain[:, cut]
+        ).astype(jnp.bfloat16)
+
+    def row_copy(spot, way, target):
+        return mesh_copy(
+            gathered.at[spot],
+            gathered.at[spot],
+            send_x.at[way, spot],
+            recv_x.at[spot],
+            "sp",
+            target,
+        )
+
+    def beside_own(way, target):
+        return mesh_copy(
+            gathered.at[place], beside.at[mine], send_b.at[way], recv_b.at[mine], "tp", target
+        )
+
+    def beside_on(o, u):
+        return mesh_copy(
+            beside.at[u], beside.at[u], send_b.at[half + o - 1], recv_b.at[u], "tp", partner
+        )
+
+    @pl.when(above)
+    def _():
+        row_copy(place, 0, me + 2).start()
+
+    @pl.when(below)
+    def _():
+        row_copy(place, 1, me - 2).start()
+
+    for o in range(1, half):
+        beside_own(o, fars(o)).start()
+    beside_own(0, partner).start()
+
+    for one, onward in zip(pair_weights(), pair_weights_on(share_at)):
+        one.wait_recv()
+        onward.start()
+    for o in range(1, half):
+        u = fars(o)
+        sd_on(o, u).wait_recv()
+        sd_on(o, u).start()
+
+    def hidden_of(block_rows, g, u):
+        gate_part = jnp.dot(block_rows, g, preferred_element_type=jnp.float32)
+        up_part = jnp.dot(block_rows, u, preferred_element_type=jnp.float32)
+        return (gate_part / (1.0 + jnp.exp(-gate_part)) * up_part).astype(jnp.bfloat16)
+
+    for i in range(1, 5):
+        loads[i].wait()
+    in_sh[mine] = hidden_of(gathered[place], s_gate[...], s_up[...])
+    in_hid[place, side] = hidden_of(gathered[place], gates[0], ups[0])
+    for one in pair_weights_on(other_at):
+        one.wait_recv()
+    in_hid[place, 1 - side] = hidden_of(gathered[place], gates[1], ups[1])
+
+    def hid_copy(spot):
+        return mesh_copy(
+            out_hid.at[spot], in_hid.at[place], send_h.at[spot], recv_h.at[place], "sp",
+            2 * spot + side,
+        )
+
+    def serve(spot):
+        out_hid[spot, side] = hidden_of(gathered[spot], gates[0], ups[0])
+        out_hid[spot, 1 - side] = hidden_of(gathered[spot], gates[1], ups[1])
+        hid_copy(spot).start()
+
+    def sh_copy(u):
+        return mesh_copy(
+            out_sh.at[u], in_sh.at[mine], send_s.at[u], recv_s.at[mine], "tp", u
+        )
+
+    def answer(u):
+        out_sh[u] = hidden_of(beside[u], s_gate[...], s_up[...])
+        sh_copy(u).start()
+
+    def pass_down(block):
+        down_pair(block).wait_recv()
+        down_pair(block).start()
+        down_core(block, core).start()
+
+    down_pair(pair).wait_recv()
+    down_core(pair, core).start()
+
+    def turn(e, carry):
+        low, high = place >= e, place + e < depth
+
+        @pl.when(low)
+        def _():
+            row_copy(place - e, 0, pair).wait_recv()
+
+            @pl.when(above)
+            def _():
+                row_copy(place - e, 0, me + 2).start()
+
+        @pl.when(high)
+        def _():
+            row_copy(place + e, 0, pair).wait_recv()
+
+            @pl.when(below)
+            def _():
+                row_copy(place + e, 1, me - 2).start()
+
+        @pl.when(low)
+        def _():
+            pass_down(me - 2 * e)
+            serve(place - e)
+
+        @pl.when(high)
+        def _():
+            pass_down(me + 2 * e)
+            serve(place + e)
+
+        @pl.when(e == 1)
+        def _():
+            for o in range(1, half):
+                u = fars(o)
+                beside_on(o, u).wait_recv()
+                beside_on(o, u).start()
+                answer(u)
+            for o in range(half):
+                u = 2 * ((far + o) % half) + 1 - core
+                beside_on(1, u).wait_recv()
+                answer(u)
+
+        return carry
+
+    lax.fori_loop(1, depth, turn, 0)
+
+    def collect(block, carry):
+        @pl.when((block % 2 != side) & (block != pair))
+        def _():
+            down_pair(block).wait_recv()
+            down_core(block, core).start()
+
+        return carry
+
+    lax.fori_loop(0, n, collect, 0)
+
+    for o in range(1, depth):
+        spot = (place + o) % depth
+        mesh_copy(
+            out_hid.at[spot], in_hid.at[spot], send_h.at[spot], recv_h.at[spot], "sp",
+            2 * spot + side,
+        ).wait_recv()
+    for o in range(1, nt):
+        u = (mine + o) % nt
+        mesh_copy(
+            out_sh.at[u], in_sh.at[u], send_s.at[u], recv_s.at[u], "tp", u
+        ).wait_recv()
+    for j in range(n):
+        units[:, j * hid : (j + 1) * hid] = (
+            in_hid[j // 2, j % 2].astype(jnp.float32) * mix[:, j : j + 1]
+        ).astype(jnp.bfloat16)
+    for j in range(nt):
+        units[:, n * hid + j * wide : n * hid + (j + 1) * wide] = in_sh[j]
+
+    loads[5].wait()
+    loads[6].wait()
+    for o in range(half):
+        sd_on(1, 2 * ((far + o) % half) + 1 - core).wait_recv()
+
+    def receive_down(block, carry):
+        @pl.when(block != me)
+        def _():
+            down_core(block, 1 - core).wait_recv()
+
+        return carry
+
+    lax.fori_loop(0, n, receive_down, 0)
+    for i in range(2 * pieces):
+        cut = slice(i * span // 2, (i + 1) * span // 2)
+        out[:, cut] = (
+            resid[:, cut].astype(jnp.float32)
+            + jnp.dot(units[...], wall[:, cut], preferred_element_type=jnp.float32)
+        ).astype(jnp.bfloat16)
+
+    def settle(e, carry):
+        @pl.when(place >= e)
+        def _():
+            block = me - 2 * e
+
+            @pl.when(above)
+            def _():
+                for one in copies(block, 0, me + 2, False):
+                    one.wait_send()
+                row_copy(place - e, 0, me + 2).wait_send()
+
+            @pl.when((e > 0) | (side == 0))
+            def _():
+                for one in copies(block, 1, pair, False):
+                    one.wait_send()
+
+        @pl.when((place + e < depth) & below)
+        def _():
+            row_copy(place + e, 1, me - 2).wait_send()
+
+        @pl.when(e != place)
+        def _():
+            hid_copy(e).wait_send()
+            down_pair(2 * e + side).wait_send()
+
+        return carry
+
+    lax.fori_loop(0, depth, settle, 0)
+
+    def settle_down(block, carry):
+        @pl.when(block != me)
+        def _():
+            down_core(block, core).wait_send()
+
+        return carry
+
+    lax.fori_loop(0, n, settle_down, 0)
+    for i in range(pieces):
+        first[i].wait_send()
+        for o in range(half - 1):
+            second[i][o].wait_send()
+    for one in pair_weights() + pair_weights_on(share_at):
+        one.wait_send()
+    for o in range(1, depth):
+        down_own(o, column(o)).wait_send()
+    down_own(0, pair).wait_send()
+    sd_own(0, partner).wait_send()
+    beside_own(0, partner).wait_send()
+    for o in range(1, half):
+        u = fars(o)
+        sd_own(o, u).wait_send()
+        sd_on(o, u).wait_send()
+        beside_own(o, u).wait_send()
+        beside_on(o, u).wait_send()
+    for o in range(1, nt):
+        sh_copy((mine + o) % nt).wait_send()
+
+
+def near(
+    stream_in,
+    q_first,
+    q_second,
+    k_first,
+    k_second,
+    values,
+    head_lambda,
+    w_out,
+    norm_gain,
+    routes,
+    route_w,
+    w_gate,
+    w_up,
+    w_down,
+    s_gate,
+    s_up,
+    s_down,
+):
+    n, nt = lax.axis_size("sp"), lax.axis_size("tp")
+    depth, half = n // 2, nt // 2
+    seq, rows, width = q_first.shape[0], stream_in.shape[0], stream_in.shape[1]
+    group, value_dim = q_first.shape[1] // HEAD, values.shape[1]
+    hid, wide = w_down.shape[1], s_down.shape[0]
+    tall, features = group * seq, group * value_dim
+    pieces = 4
+    span = width // pieces
+    chosen = routes[:, :, None] == jnp.arange(n, dtype=jnp.int32)[None, None, :]
+    mix = jnp.sum(jnp.where(chosen, route_w[:, :, None], 0.0), axis=1)
+    vmem = pl.BlockSpec(memory_space=pltpu.VMEM)
+    smem = pl.BlockSpec(memory_space=pltpu.SMEM)
+    hbm = pl.BlockSpec(memory_space=pl.ANY)
+    low, high = jnp.bfloat16, jnp.float32
+    dma = pltpu.SemaphoreType.DMA
+    return pl.pallas_call(
+        functools.partial(near_kernel, n, nt, group, pieces),
+        out_shape=jax.ShapeDtypeStruct((rows, width), low),
+        in_specs=[vmem] * 5 + [smem, hbm] + [vmem] * 3 + [hbm] * 6,
+        out_specs=vmem,
+        scratch_shapes=[
+            pltpu.VMEM((2, tall, HEAD), low),
+            pltpu.VMEM((n, seq, HEAD), low),
+            pltpu.VMEM((n, seq, HEAD), low),
+            pltpu.VMEM((n, seq, value_dim), low),
+            pltpu.VMEM((2, tall, 1), high),
+            pltpu.VMEM((2, tall, 1), high),
+            pltpu.VMEM((2, tall, value_dim), high),
+            pltpu.VMEM((seq, features), low),
+            pltpu.VMEM((features, width), low),
+            pltpu.VMEM((2, half * rows, features), low),
+            pltpu.VMEM((pieces, half * rows, span), low),
+            pltpu.VMEM((pieces, half * rows, span), low),
+            pltpu.VMEM((half - 1, pieces, rows, span), low),
+            pltpu.VMEM((half - 1, pieces, rows, span), low),
+            pltpu.VMEM((rows, width), low),
+            pltpu.VMEM((2, width, hid), low),
+            pltpu.VMEM((2, width, hid), low),
+            pltpu.VMEM((width, wide), low),
+            pltpu.VMEM((width, wide), low),
+            pltpu.VMEM((n * hid + nt * wide, width), low),
+            pltpu.VMEM((depth, rows, width), low),
+            pltpu.VMEM((nt, rows, width), low),
+            pltpu.VMEM((depth, 2, rows, hid), low),
+            pltpu.VMEM((depth, 2, rows, hid), low),
+            pltpu.VMEM((nt, rows, wide), low),
+            pltpu.VMEM((nt, rows, wide), low),
+            pltpu.VMEM((rows, n * hid + nt * wide), low),
+            dma((7,)),
+            dma((2, 3, n)),
+            dma((3, n)),
+            dma((pieces,)),
+            dma((pieces,)),
+            dma((half - 1, pieces)),
+            dma((half - 1, pieces)),
+            dma((2, 2)),
+            dma((2, 2)),
+            dma((depth + 2 * n,)),
+            dma((2, n)),
+            dma((nt,)),
+            dma((nt,)),
+            dma((2, depth)),
+            dma((depth,)),
+            dma((nt,)),
+            dma((nt,)),
+            dma((depth,)),
+            dma((depth,)),
+            dma((nt,)),
+            dma((nt,)),
+        ],
+        compiler_params=pltpu.CompilerParams(
+            collective_id=0, has_side_effects=True, vmem_limit_bytes=60 << 20
+        ),
+        name="layer",
+    )(
+        q_first, q_second, k_first, k_second, values, head_lambda, w_out, stream_in,
+        norm_gain.reshape(1, width), mix, w_gate[0], w_up[0], s_gate, s_up, w_down[0], s_down,
+    )
+
+
+def layer(*arrays):
+    n, nt = lax.axis_size("sp"), lax.axis_size("tp")
+    k_first, values, w_gate, w_down, s_down = (arrays[i] for i in (3, 5, 11, 13, 16))
+    fits = (
+        2 <= n <= 16
+        and n % 2 == 0
+        and nt >= 4
+        and nt % 2 == 0
+        and k_first.shape[1] == HEAD
+        and w_gate.shape[0] == 1
+        and w_down.shape[1] % (16 * nt) == 0
+        and s_down.shape[0] % (16 * n) == 0
+    )
+    return near(*arrays) if fits else local(*arrays)
+
+
 def solution(mesh):
     return jax.shard_map(
-        local,
+        layer,
         mesh=mesh,
         in_specs=(
             P(("sp", "tp"), None),

time: 314 us -> 123 us (0.39)
  the two profiles are of different devices: /device:TPU:0 before, /device:TPU:27 now
where the time goes in v2:
time: 123 us
  Pallas kernels  120 us (98%)
  local copies, waits for them, and re-layouts  2.57 us (2%)
    pallas_call x1, Pallas kernels, near(): pl.pallas_call(functools.partial(near_kernel, n, nt, group, pieces), out_...  120 us

profile of v2, /device:TPU:27, one launch (start us, length us, event | category | flops | bytes accessed | tf_op | source)
XLA Modules:
  0.0 123.3 jit_solution(15003071993501269944)
XLA Ops:
  0.0 0.7 select_reduce_fusion
  0.7 0.7 copy.20.mix
  1.4 120.0 %layer.1 = bf16[64,4096]{1,0:T(8,128)(2,1)} custom-call(bf16[256,256]{1,0:T(8,128)(2,1)} %q_one.1, bf16[256,256]{1,0:T(8,128)(2,1)} %q_two.1, bf16[256,128]{1,0:T(8,128)(2,1)} %k_one.1, bf16[256,128]{1,0:T(8,128)(2,1)} %k_two.1, bf16[256,256]{1,0:T(8,128)(2,1)} %val.1, f32[2]{0:T(128)} %lam.1, bf16[512,4096]{1,0:T(8,128)(2,1)} %w_out_h.1, ...), custom_call_target="tpu_custom_call" | custom-call | tf_op jit(solution)/shard_map/layer/pallas_call | solution.py:794
  121.4 1.9 %copy.22 = bf16[64,4096]{1,0:T(8,128)(2,1)} copy(bf16[64,4096]{1,0:T(8,128)(2,1)} %layer.1) | data formatting | bytes 1048576

commit v3 on v2

--- a/solution.py
+++ b/solution.py
@@ -450,11 +450,25 @@
 
     lax.fori_loop(1, depth + 1, visit, 0)
 
-    for o in range(1, depth):
-
-        @pl.when(place + o < depth)
-        def _():
-            down_own(o, column(o)).start()
+    @pl.when(above)
+    def _():
+        down_own(1, me + 2).start()
+
+    def down_up(block):
+        return mesh_copy(
+            down_at(block, core),
+            down_at(block, core),
+            send_d.at[depth + 2 * n + block],
+            recv_d.at[0, block],
+            "sp",
+            me + 2,
+        )
+
+    def lift(d):
+        @pl.when((place >= d) & above)
+        def _():
+            down_up(me - 2 * d).wait_recv()
+            down_up(me - 2 * d).start()
 
     for h in range(group):
         cut = slice(h * seq, (h + 1) * seq)
@@ -496,6 +510,7 @@
             order[0], w[:, i * span : (i + 1) * span], preferred_element_type=jnp.float32
         ).astype(jnp.bfloat16)
         first[i].start()
+    lift(1)
     kept = []
     for i in range(pieces):
         sums = jnp.dot(
@@ -507,6 +522,12 @@
             out_two[o, i] = sums[(o + 1) * rows : (o + 2) * rows].astype(jnp.bfloat16)
             second[i][o].start()
         kept.append(sums[:rows])
+    for d in range(2, depth):
+        lift(d)
+    for o in range(1, half):
+        u = fars(o)
+        sd_on(o, u).wait_recv()
+        sd_on(o, u).start()
     squares = jnp.zeros((rows, 1), jnp.float32)
     for i in range(pieces):
         cut = slice(i * span, (i + 1) * span)
@@ -525,12 +546,15 @@
             resid[:, cut].astype(jnp.float32) * shrink * gain[:, cut]
         ).astype(jnp.bfloat16)
 
-    def row_copy(spot, way, target):
+    chunk = rows // 2
+
+    def row_copy(spot, way, target, c):
+        some = gathered.at[spot, pl.ds(c * chunk, chunk)]
         return mesh_copy(
-            gathered.at[spot],
-            gathered.at[spot],
-            send_x.at[way, spot],
-            recv_x.at[spot],
+            some,
+            some,
+            send_x.at[way, c, spot],
+            recv_x.at[c, spot],
             "sp",
             target,
         )
@@ -545,26 +569,35 @@
             beside.at[u], beside.at[u], send_b.at[half + o - 1], recv_b.at[u], "tp", partner
         )
 
-    @pl.when(above)
-    def _():
-        row_copy(place, 0, me + 2).start()
-
-    @pl.when(below)
-    def _():
-        row_copy(place, 1, me - 2).start()
+    for c in range(2):
+        pl.when(above)(lambda: row_copy(place, 0, me + 2, c).start())
+        pl.when(below)(lambda: row_copy(place, 1, me - 2, c).start())
 
     for o in range(1, half):
         beside_own(o, fars(o)).start()
     beside_own(0, partner).start()
 
+    def pass_down(e):
+        def one(block, fresh):
+            pl.when(fresh)(lambda: down_pair(block).wait_recv())
+            down_pair(block).start()
+            down_core(block, core).start()
+
+        pl.when(place >= e)(lambda: one(me - 2 * e, jnp.logical_not(above)))
+        pl.when(place + e < depth)(lambda: one(me + 2 * e, place >= 0))
+
+    def collect(e):
+        def one(block):
+            down_pair(block).wait_recv()
+            down_core(block, core).start()
+
+        pl.when(place >= e)(lambda: one(pair - 2 * e))
+        pl.when(place + e < depth)(lambda: one(pair + 2 * e))
+
     for one, onward in zip(pair_weights(), pair_weights_on(share_at)):
         one.wait_recv()
         onward.start()
-    for o in range(1, half):
-        u = fars(o)
-        sd_on(o, u).wait_recv()
-        sd_on(o, u).start()
-
+    pass_down(1)
     def hidden_of(block_rows, g, u):
         gate_part = jnp.dot(block_rows, g, preferred_element_type=jnp.float32)
         up_part = jnp.dot(block_rows, u, preferred_element_type=jnp.float32)
@@ -574,9 +607,6 @@
         loads[i].wait()
     in_sh[mine] = hidden_of(gathered[place], s_gate[...], s_up[...])
     in_hid[place, side] = hidden_of(gathered[place], gates[0], ups[0])
-    for one in pair_weights_on(other_at):
-        one.wait_recv()
-    in_hid[place, 1 - side] = hidden_of(gathered[place], gates[1], ups[1])
 
     def hid_copy(spot):
         return mesh_copy(
@@ -598,45 +628,45 @@
         out_sh[u] = hidden_of(beside[u], s_gate[...], s_up[...])
         sh_copy(u).start()
 
-    def pass_down(block):
-        down_pair(block).wait_recv()
-        down_pair(block).start()
-        down_core(block, core).start()
-
-    down_pair(pair).wait_recv()
-    down_core(pair, core).start()
-
     def turn(e, carry):
         low, high = place >= e, place + e < depth
 
+        for c in range(2):
+
+            @pl.when(low)
+            def _():
+                row_copy(place - e, 0, pair, c).wait_recv()
+                pl.when(above)(lambda: row_copy(place - e, 0, me + 2, c).start())
+
+            @pl.when(high)
+            def _():
+                row_copy(place + e, 0, pair, c).wait_recv()
+                pl.when(below)(lambda: row_copy(place + e, 1, me - 2, c).start())
+
+        pass_down(e + 1)
+
+        @pl.when(e == 1)
+        def _():
+            down_pair(pair).wait_recv()
+            down_core(pair, core).start()
+            for one in pair_weights_on(other_at):
+                one.wait_recv()
+
         @pl.when(low)
         def _():
-            row_copy(place - e, 0, pair).wait_recv()
-
-            @pl.when(above)
-            def _():
-                row_copy(place - e, 0, me + 2).start()
+            serve(place - e)
 
         @pl.when(high)
         def _():
-            row_copy(place + e, 0, pair).wait_recv()
-
-            @pl.when(below)
-            def _():
-                row_copy(place + e, 1, me - 2).start()
-
-        @pl.when(low)
-        def _():
-            pass_down(me - 2 * e)
-            serve(place - e)
-
-        @pl.when(high)
-        def _():
-            pass_down(me + 2 * e)
             serve(place + e)
 
+        @pl.when(e > 1)
+        def _():
+            collect(e - 1)
+
         @pl.when(e == 1)
         def _():
+            in_hid[place, 1 - side] = hidden_of(gathered[place], gates[1], ups[1])
             for o in range(1, half):
                 u = fars(o)
                 beside_on(o, u).wait_recv()
@@ -651,15 +681,7 @@
 
     lax.fori_loop(1, depth, turn, 0)
 
-    def collect(block, carry):
-        @pl.when((block % 2 != side) & (block != pair))
-        def _():
-            down_pair(block).wait_recv()
-            down_core(block, core).start()
-
-        return carry
-
-    lax.fori_loop(0, n, collect, 0)
+    collect(depth - 1)
 
     for o in range(1, depth):
         spot = (place + o) % depth
@@ -708,7 +730,12 @@
             def _():
                 for one in copies(block, 0, me + 2, False):
                     one.wait_send()
-                row_copy(place - e, 0, me + 2).wait_send()
+                for c in range(2):
+                    row_copy(place - e, 0, me + 2, c).wait_send()
+
+                @pl.when(e > 0)
+                def _():
+                    down_up(block).wait_send()
 
             @pl.when((e > 0) | (side == 0))
             def _():
@@ -717,7 +744,8 @@
 
         @pl.when((place + e < depth) & below)
         def _():
-            row_copy(place + e, 1, me - 2).wait_send()
+            for c in range(2):
+                row_copy(place + e, 1, me - 2, c).wait_send()
 
         @pl.when(e != place)
         def _():
@@ -743,7 +771,7 @@
     for one in pair_weights() + pair_weights_on(share_at):
         one.wait_send()
     for o in range(1, depth):
-        down_own(o, column(o)).wait_send()
+        pl.when((place + o >= depth) | (o == 1))(lambda: down_own(o, column(o)).wait_send())
     down_own(0, pair).wait_send()
     sd_own(0, partner).wait_send()
     beside_own(0, partner).wait_send()
@@ -833,12 +861,12 @@
             dma((half - 1, pieces)),
             dma((2, 2)),
             dma((2, 2)),
-            dma((depth + 2 * n,)),
+            dma((depth + 3 * n,)),
             dma((2, n)),
             dma((nt,)),
             dma((nt,)),
+            dma((2, 2, depth)),
             dma((2, depth)),
-            dma((depth,)),
             dma((nt,)),
             dma((nt,)),
             dma((depth,)),

time: 123 us -> 111 us (0.902)
  the two profiles are of different devices: /device:TPU:27 before, /device:TPU:0 now
where the time goes in v3:
time: 111 us
  Pallas kernels  108 us (97%)
  local copies, waits for them, and re-layouts  2.57 us (2%)
    pallas_call x1, Pallas kernels, near(): pl.pallas_call(functools.partial(near_kernel, n, nt, group, pieces), out_...  108 us

profile of v3, /device:TPU:0, one launch (start us, length us, event | category | flops | bytes accessed | tf_op | source)
XLA Modules:
  0.0 111.1 jit_solution(7398015712126830968)
XLA Ops:
  0.0 0.7 select_reduce_fusion
  0.7 0.7 copy.20.mix
  1.4 107.8 %layer.1 = bf16[64,4096]{1,0:T(8,128)(2,1)} custom-call(bf16[256,256]{1,0:T(8,128)(2,1)} %q_one.1, bf16[256,256]{1,0:T(8,128)(2,1)} %q_two.1, bf16[256,128]{1,0:T(8,128)(2,1)} %k_one.1, bf16[256,128]{1,0:T(8,128)(2,1)} %k_two.1, bf16[256,256]{1,0:T(8,128)(2,1)} %val.1, f32[2]{0:T(128)} %lam.1, bf16[512,4096]{1,0:T(8,128)(2,1)} %w_out_h.1, ...), custom_call_target="tpu_custom_call" | custom-call | tf_op jit(solution)/shard_map/layer/pallas_call | solution.py:822
  109.2 1.9 %copy.22 = bf16[64,4096]{1,0:T(8,128)(2,1)} copy(bf16[64,4096]{1,0:T(8,128)(2,1)} %layer.1) | data formatting | bytes 1048576
